TPU v7x, 32 devices: a whole 2x2x4 slice. The times are simulated.
32 devices in a mesh: sp: 4 (over y, core), tp: 8 (over z, x).
Axes of the slice: x: 2, y: 2, z: 4, core: 2. Of those that a mesh axis runs over, the one named last changes fastest.
Arguments:
- latent: bfloat16 [960, 2048], P(('sp', 'tp')), may hold values from -40 to 40
- context: bfloat16 [768, 2048], P('sp'), may hold values from -6 to 6
- cond_latent: float32 [2048], P('sp'), may hold values from -6 to 6
- cond_context: float32 [2048], P('sp'), may hold values from -6 to 6
- mod_weight: bfloat16 [2048, 6144], P('sp', 'tp'), may hold values from -0.125 to 0.125
- w_query: bfloat16 [2048, 1024], P(None, 'tp'), may hold values from -5 to 5
- w_key: bfloat16 [2048, 1024], P(None, 'tp'), may hold values from -5 to 5
- w_value: bfloat16 [2048, 1024], P(None, 'tp'), may hold values from -0.125 to 0.125
- w_out: bfloat16 [1024, 2048], P('tp'), may hold values from -0.1875 to 0.1875
- head_lambda: float32 [8], P('tp'), may hold values from 0.3 to 0.8
Outputs:
- mixed_latent: bfloat16 [960, 2048], P(('sp', 'tp'))
All inputs are finite; a program needn't handle non-finite values.
Results may differ from a plain program's by a relative error of at most 0.011.
Values may be sent and summed in bfloat16 or wider, within the bound.
A program may use at most 64 MiB of HBM per device.

v0:
```python
import jax
import jax.numpy as jnp
from jax import lax
from jax.sharding import PartitionSpec as P

QK_DIM = 64
VAL_DIM = 128
GRID_W = 64
NORM_EPS = 0.01
HEAD_EPS = 0.001
THETA = 10000.0


def modulate_rows(rows, shift, scale):
    values = rows.astype(jnp.float32)
    normed = values * lax.rsqrt(jnp.mean(values * values, axis=-1, keepdims=True) + NORM_EPS)
    return (normed * (1.0 + scale) + shift).astype(jnp.bfloat16)


def rotary_tables(positions):
    quarter = QK_DIM // 4
    inverse = THETA ** (-jnp.arange(quarter, dtype=jnp.float32) / quarter)
    grid_row = (positions // GRID_W).astype(jnp.float32)
    grid_column = (positions % GRID_W).astype(jnp.float32)
    by_row = grid_row[:, None] * inverse[None, :]
    by_column = grid_column[:, None] * inverse[None, :]
    angle = jnp.concatenate([by_row, by_row, by_column, by_column], axis=-1)
    return (jnp.cos(angle), jnp.sin(angle))


def rotate(product, cosine, sine):
    number = product.shape[0]
    quarter = QK_DIM // 4
    half = QK_DIM // 2
    shaped = product.reshape(number, -1, QK_DIM)
    first = shaped[..., :half]
    second = shaped[..., half:]
    turned = jnp.concatenate(
        [
            -first[..., quarter:],
            first[..., :quarter],
            -second[..., quarter:],
            second[..., :quarter],
        ],
        axis=-1,
    )
    result = shaped * cosine[:, None, :] + turned * sine[:, None, :]
    return result.reshape(number, -1).astype(jnp.bfloat16)


def attend_piece(state, piece, queries):
    highest, totals, carried = state
    keys, values = piece
    number = keys.shape[0]
    heads = queries.shape[1]
    key_heads = keys.reshape(number, heads, 2, QK_DIM)
    value_heads = values.reshape(number, heads, VAL_DIM)
    scores = jnp.einsum(
        "qhmd,khmd->hmqk", queries, key_heads, preferred_element_type=jnp.float32
    ) * QK_DIM ** (-0.5)
    new_highest = jnp.maximum(highest, jnp.max(scores, axis=-1))
    weights = jnp.exp(scores - new_highest[..., None])
    totals = jnp.sum(weights, axis=-1)
    mixed = jnp.einsum(
        "hmqk,khd->hmqd",
        weights.astype(jnp.bfloat16),
        value_heads,
        preferred_element_type=jnp.float32,
    )
    carried = mixed
    return (new_highest, totals, carried)


def shards(
    latent,
    context,
    cond_latent,
    cond_context,
    mod_weight,
    w_query,
    w_key,
    w_value,
    w_out,
    head_lambda,
):
    width = latent.shape[1]
    heads = head_lambda.shape[0]
    conditioned = jax.nn.silu(jnp.stack([cond_latent, cond_context])).astype(jnp.bfloat16)
    partial_mod = jnp.dot(conditioned, mod_weight, preferred_element_type=jnp.float32)
    summed = lax.psum(partial_mod, "sp")
    modulation = lax.all_gather(summed, "tp", axis=1, tiled=True)
    shift_context = modulation[1, :width]
    scale_context = modulation[1, width : 2 * width]
    gate_latent = modulation[0, 2 * width :]
    own_rows = modulate_rows(latent, modulation[0, :width], modulation[0, width : 2 * width])
    group_rows = latent.shape[0] * lax.axis_size("tp")
    offset = lax.axis_index("sp") * group_rows
    piece = lax.all_gather(own_rows, "tp", axis=0, tiled=True)
    positions = offset + jnp.arange(piece.shape[0], dtype=jnp.int32)
    cosine, sine = rotary_tables(positions)
    query_part = rotate(jnp.dot(piece, w_query, preferred_element_type=jnp.float32), cosine, sine)
    key_part = rotate(jnp.dot(piece, w_key, preferred_element_type=jnp.float32), cosine, sine)
    value_part = jnp.dot(piece, w_value, preferred_element_type=jnp.float32).astype(jnp.bfloat16)
    projected = jnp.concatenate([query_part, key_part, value_part], axis=1)
    key_columns = heads * 2 * QK_DIM
    queries = projected[:, :key_columns].reshape(group_rows, heads, 2, QK_DIM)
    keys = projected[:, key_columns : 2 * key_columns]
    values = projected[:, 2 * key_columns :]
    initial = (
        jnp.full((heads, 2, group_rows), -1e30, jnp.float32),
        jnp.zeros((heads, 2, group_rows), jnp.float32),
        jnp.zeros((heads, 2, group_rows, VAL_DIM), jnp.float32),
    )
    own_context = modulate_rows(context, shift_context, scale_context)
    context_keys = jnp.dot(own_context, w_key, preferred_element_type=jnp.float32).astype(
        jnp.bfloat16
    )
    context_values = jnp.dot(own_context, w_value, preferred_element_type=jnp.float32).astype(
        jnp.bfloat16
    )
    joined_keys = jnp.concatenate([keys, context_keys], axis=0)
    joined_values = jnp.concatenate([values, context_values], axis=0)
    state = attend_piece(
        initial,
        (
            lax.all_gather(joined_keys, "sp", axis=0, tiled=True),
            lax.all_gather(joined_values, "sp", axis=0, tiled=True),
        ),
        queries,
    )
    highest, totals, carried = state
    factor = head_lambda[:, None, None]
    head_out = (
        carried[:, 0] / totals[:, 0][..., None] - factor * carried[:, 1] / totals[:, 1][..., None]
    )
    head_out = head_out * lax.rsqrt(
        jnp.mean(head_out * head_out, axis=-1, keepdims=True) + HEAD_EPS
    )
    attended = (
        jnp.transpose(head_out, (1, 0, 2)).reshape(group_rows, heads * VAL_DIM).astype(jnp.bfloat16)
    )
    branch = lax.psum_scatter(
        jnp.dot(attended, w_out, preferred_element_type=jnp.float32),
        "tp",
        scatter_dimension=0,
        tiled=True,
    )
    branch = branch * lax.rsqrt(jnp.mean(branch * branch, axis=-1, keepdims=True) + NORM_EPS)
    return (latent.astype(jnp.float32) + gate_latent * branch).astype(jnp.bfloat16)


def solution(mesh):
    placed = (
        P(("sp", "tp"), None),
        P("sp", None),
        P("sp"),
        P("sp"),
        P("sp", "tp"),
        P(None, "tp"),
        P(None, "tp"),
        P(None, "tp"),
        P("tp", None),
        P("tp"),
    )
    return jax.shard_map(
        shards, mesh=mesh, in_specs=placed, out_specs=P(("sp", "tp"), None), check_vma=False
    )
```

profile of v0, /device:TPU:8, one launch (start us, length us, event | category | flops | bytes accessed | tf_op | source)
XLA Modules:
  0.0 153.3 jit_solution(12564381263375404381)
XLA Ops:
  0.0 1.1 fusion.14
  1.2 1.5 fusion.6
  2.7 0.9 fusion.37
  3.6 7.0 %psum.7 = f32[2,768]{1,0:T(2,128)S(1)} all-reduce(f32[2,768]{1,0:T(2,128)S(1)} %fusion.37), channel_id=1, replica_groups=mesh['sp'=4,'tp'=8] {'sp'}, use_global_device_ids=true, to_apply=%region_0.1 | all-reduce | flops 1536 | bytes 12288 | tf_op jit(solution)/shard_map/psum | solution.py:90
  10.6 28.2 %all_gather.12 = f32[2,6144]{1,0:T(2,128)S(1)} all-gather(f32[2,768]{1,0:T(2,128)S(1)} %psum.7), channel_id=1, replica_groups=mesh['sp'=4,'tp'=8] {'tp'}, dimensions={1}, use_global_device_ids=true | all-gather | bytes 55296 | tf_op jit(solution)/shard_map/all_gather | solution.py:91
  38.9 1.8 %convolution_convert_fusion.1 = bf16[192,128]{1,0:T(8,128)(2,1)S(1)} fusion(bf16[2048,128]{1,0:T(8,128)(2,1)} %param.17, bf16[192,2048]{1,0:T(8,128)(2,1)} %param.11, f32[2048]{0:T(1024)S(1)} %bitcast.84, f32[2048]{0:T(1024)S(1)} %bitcast.86, f32[192]{0:T(256)S(1)} %add_rsqrt_fusion.1), kind=kOutput, calls=%fused_computation.14 | convolution fusion | flops 102653952 | bytes 1377024 | tf_op jit(solution)/shard_map/dot_general | solution.py:118
  40.7 0.5 convolution_convert_fusion.2
  41.2 0.1 fusion.19
  41.3 33.0 %all-gather = bf16[8,30,2048]{2,1,0:T(8,128)(2,1)S(1)} all-gather(bf16[1,30,2048]{2,1,0:T(8,128)(2,1)S(1)} %fusion.19), channel_id=1, replica_groups=mesh['sp'=4,'tp'=8] {'tp'}, dimensions={0}, use_global_device_ids=true | all-gather | bytes 1105920 | tf_op jit(solution)/shard_map/all_gather | solution.py:98
  74.3 0.3 reshape.355
  74.6 1.5 convolution_convert_fusion
  76.1 1.4 fusion.49
  78.3 0.1 fusion.35
  78.5 0.4 fusion.48
  78.9 0.1 copy.22
  79.5 0.1 copy.24
  79.6 6.3 %all_gather.14 = bf16[1728,128]{1,0:T(8,128)(2,1)S(1)} all-gather(bf16[432,128]{1,0:T(8,128)(2,1)S(1)} %pad_maximum_fusion), channel_id=1, replica_groups=mesh['sp'=4,'tp'=8] {'sp'}, dimensions={0}, use_global_device_ids=true | all-gather | bytes 552960 | tf_op jit(solution)/shard_map/all_gather | solution.py:126
  85.9 0.2 copy.28
  86.1 6.8 %all_gather.15 = bf16[1728,128]{1,0:T(8,128)(2,1)S(1)} all-gather(bf16[432,128]{1,0:T(8,128)(2,1)S(1)} %pad_maximum_fusion.1), channel_id=1, replica_groups=mesh['sp'=4,'tp'=8] {'sp'}, dimensions={0}, use_global_device_ids=true | all-gather | bytes 552960 | tf_op jit(solution)/shard_map/all_gather | solution.py:127
  92.9 0.7 fusion.47
  93.7 0.6 fusion.1
  94.3 0.7 fusion.10
  95.0 0.2 fusion.27
  95.2 0.1 copy-done.5
  95.3 0.5 fusion.28
  95.8 48.5 %fusion = f32[32,2048]{1,0:T(8,128)S(1)} fusion(f32[240,2048]{1,0:T(8,128)S(1)} %fusion.28), kind=kCustom, calls=%all-reduce-scatter | all-reduce-scatter fusion | flops 524289 | bytes 2228736
  144.3 4.3 %collective-permute-start = (f32[14,2048]{1,0:T(8,128)S(1)}, f32[14,2048]{1,0:T(8,128)S(1)}, u32[]{:S(2)}, u32[]{:S(2)}) collective-permute-start(f32[14,2048]{1,0:T(8,128)S(1)} %slice.97), channel_id=1, source_target_pairs={{0,1},{1,2},{2,3},{3,4},{4,5},{5,6},{6,7},{8,9},{9,10},{10,11},{11... | collective-permute-start | bytes 344072
  148.6 0.6 dynamic-slice.4
  149.9 2.2 %collective-permute-done = f32[14,2048]{1,0:T(8,128)S(1)} collective-permute-done((f32[14,2048]{1,0:T(8,128)S(1)}, f32[14,2048]{1,0:T(8,128)S(1)}, u32[]{:S(2)}, u32[]{:S(2)}) %collective-permute-start) | collective-permute-done | bytes 114720
  152.1 0.2 concatenate.28
  152.4 0.2 multiply_reduce_fusion
  152.5 0.8 fusion.18
  (34 shorter events, 0.7 us)
Async XLA Ops:
  0.0 2.6 %copy-start = (bf16[512,768]{1,0:T(8,128)(2,1)S(1)}, bf16[512,768]{1,0:T(8,128)(2,1)}, u32[]{:S(2)}) copy-start(bf16[512,768]{1,0:T(8,128)(2,1)} %param.14) | copy-start | bytes 2359300
  1.1 39.6 %copy-start.2 = (bf16[192,2048]{1,0:T(8,128)(2,1)S(1)}, bf16[192,2048]{1,0:T(8,128)(2,1)}, u32[]{:S(2)}) copy-start(bf16[192,2048]{1,0:T(8,128)(2,1)} %param.11) | copy-start | bytes 2359300
  1.2 39.5 %copy-start.3 = (bf16[2048,128]{1,0:T(8,128)(2,1)S(1)}, bf16[2048,128]{1,0:T(8,128)(2,1)}, u32[]{:S(2)}) copy-start(bf16[2048,128]{1,0:T(8,128)(2,1)} %param.16) | copy-start | bytes 1572868
  38.9 2.3 %copy-start.1 = (bf16[30,2048]{1,0:T(8,128)(2,1)S(1)}, bf16[30,2048]{1,0:T(8,128)(2,1)}, u32[]{:S(2)}) copy-start(bf16[30,2048]{1,0:T(8,128)(2,1)} %param.10) | copy-start | bytes 368644
  74.6 4.0 %copy-start.4 = (bf16[2048,128]{1,0:T(8,128)(2,1)S(1)}, bf16[2048,128]{1,0:T(8,128)(2,1)}, u32[]{:S(2)}) copy-start(bf16[2048,128]{1,0:T(8,128)(2,1)} %param.15) | copy-start | bytes 1572868
  94.3 1.0 copy-start.5
  95.3 53.3 %copy-start.6 = (u32[32]{0:T(128)S(1)}, u32[32]{0:T(128)}, u32[]{:S(2)}) copy-start(u32[32]{0:T(128)} %constant.70) | copy-start | bytes 388
  144.3 7.8 %collective-permute-start = (f32[14,2048]{1,0:T(8,128)S(1)}, f32[14,2048]{1,0:T(8,128)S(1)}, u32[]{:S(2)}, u32[]{:S(2)}) collective-permute-start(f32[14,2048]{1,0:T(8,128)S(1)} %slice.97), channel_id=1, source_target_pairs={{0,1},{1,2},{2,3},{3,4},{4,5},{5,6},{6,7},{8,9},{9,10},{10,11},{11... | collective-permute-start | bytes 344072
where the time goes:
time: 154 us; the launch traced here: 153 us
  blocking collectives  130 us (84%)
  matrix products  8.4 us (5%)
  other arithmetic  4.88 us (3%)
  starting transfers between devices  4.27 us (3%)
  waiting for transfers between devices  2.24 us (1%)
  local copies, waits for them, and re-layouts  2.05 us (1%)
  between operations  1.61 us (1%)
    unnamed x1, blocking collectives  48.5 us
    all_gather x1, blocking collectives, shards(): piece = lax.all_gather(own_rows, 'tp', axis=0, tiled=True)  33 us
    all_gather x1, blocking collectives, shards(): modulation = lax.all_gather(summed, 'tp', axis=1, tiled=True)  28.2 us
    psum x1, blocking collectives, shards(): summed = lax.psum(partial_mod, 'sp')  7.04 us
    all_gather x1, blocking collectives, shards(): lax.all_gather(joined_values, 'sp', axis=0, tiled=True)  6.83 us
    all_gather x1, blocking collectives, shards(): lax.all_gather(joined_keys, 'sp', axis=0, tiled=True)  6.28 us
    unnamed x1, starting transfers between devices  4.27 us
  transfers between devices with their start and end apart: 1, of which 1 were waited for; matrix products, arithmetic and copies ran while one was open for 0% of the time, Pallas kernels for 0%

commit v1 on v0

--- a/solution.py
+++ b/solution.py
@@ -88,7 +88,8 @@
     conditioned = jax.nn.silu(jnp.stack([cond_latent, cond_context])).astype(jnp.bfloat16)
     partial_mod = jnp.dot(conditioned, mod_weight, preferred_element_type=jnp.float32)
     summed = lax.psum(partial_mod, "sp")
-    modulation = lax.all_gather(summed, "tp", axis=1, tiled=True)
+    repeated = jnp.stack([summed] * lax.axis_size("tp"))
+    modulation = jnp.concatenate(lax.all_to_all(repeated, "tp", 0, 0), axis=1)
     shift_context = modulation[1, :width]
     scale_context = modulation[1, width : 2 * width]
     gate_latent = modulation[0, 2 * width :]

time: 154 us -> 132 us (0.86)
  blocking collectives: 130 us -> 99.6 us
  starting transfers between devices: 4.27 us -> 8.17 us
  waiting for transfers between devices: 2.24 us -> 6.14 us
  local copies, waits for them, and re-layouts: 2.05 us -> 3.8 us
    all_gather x1 -> x0, blocking collectives: 28.2 us -> none  [shards(): modulation = lax.all_gather(summed, 'tp', axis=1, tiled=True)]
    all_to_all x0 -> x1, starting transfers between devices: none -> 6.25 us  [shards(): modulation = jnp.concatenate(lax.all_to_all(repeated, 'tp', 0, 0), axis=1)]
    unnamed x1, starting transfers between devices: 4.27 us -> 1.92 us
    unnamed x1, waiting for transfers between devices: 2.24 us -> 4.58 us
    all_gather x1, blocking collectives: 33 us -> 31.1 us  [shards(): piece = lax.all_gather(own_rows, 'tp', axis=0, tiled=True)]
    all_to_all x0 -> x1, waiting for transfers between devices: none -> 1.55 us  [shards(): modulation = jnp.concatenate(lax.all_to_all(repeated, 'tp', 0, 0), axis=1)]
  transfers between devices with their start and end apart: 1 -> 2, of which waited for: 1 -> 2; matrix products, arithmetic and copies ran while one was open for 0% -> 3% of each run, Pallas kernels for 0% -> 0%
where the time goes in v1:
time: 132 us; the launch traced here: 131 us
  blocking collectives  99.6 us (75%)
  starting transfers between devices  8.17 us (6%)
  matrix products  7.1 us (5%)
  waiting for transfers between devices  6.14 us (5%)
  other arithmetic  4.77 us (4%)
  local copies, waits for them, and re-layouts  3.8 us (3%)
  between operations  1.62 us (1%)
    unnamed x1, blocking collectives  48.4 us
    all_gather x1, blocking collectives, shards(): piece = lax.all_gather(own_rows, 'tp', axis=0, tiled=True)  31.1 us
    psum x1, blocking collectives, shards(): summed = lax.psum(partial_mod, 'sp')  7.04 us
    all_gather x1, blocking collectives, shards(): lax.all_gather(joined_values, 'sp', axis=0, tiled=True)  6.83 us
    all_gather x1, blocking collectives, shards(): lax.all_gather(joined_keys, 'sp', axis=0, tiled=True)  6.28 us
    all_to_all x1, starting transfers between devices, shards(): modulation = jnp.concatenate(lax.all_to_all(repeated, 'tp', 0, 0), axis=1)  6.25 us
    unnamed x1, waiting for transfers between devices  4.58 us
  transfers between devices with their start and end apart: 2, of which 2 were waited for; matrix products, arithmetic and copies ran while one was open for 3% of the time, Pallas kernels for 0%

profile of v1, /device:TPU:8, one launch (start us, length us, event | category | flops | bytes accessed | tf_op | source)
XLA Modules:
  0.0 131.2 jit_solution(12008951585253511056)
XLA Ops:
  0.0 1.1 copy-done
  1.1 0.9 fusion.37
  2.0 7.0 %psum.7 = f32[2,768]{1,0:T(2,128)S(1)} all-reduce(f32[2,768]{1,0:T(2,128)S(1)} %fusion.37), channel_id=1, replica_groups=mesh['sp'=4,'tp'=8] {'sp'}, use_global_device_ids=true, to_apply=%region_0.1 | all-reduce | flops 1536 | bytes 12288 | tf_op jit(solution)/shard_map/psum | solution.py:90
  9.1 0.6 stack.11
  9.7 6.3 %all-to-all-start = ((f32[8,2,768]{2,1,0:T(2,128)}), f32[8,2,768]{2,1,0:T(2,128)S(1)}, u32[]{:S(2)}, u32[]{:S(2)}) async-start(f32[8,2,768]{2,1,0:T(2,128)} %stack.11), calls=%async_computation | async-start | bytes 98304 | tf_op jit(solution)/shard_map/all_to_all | solution.py:92
  16.7 1.1 fusion.14
  17.8 1.4 %fusion.6 = f32[192]{0:T(256)S(1)} fusion(bf16[192,2048]{1,0:T(8,128)(2,1)} %param.11), kind=kLoop, calls=%fused_computation.8 | loop fusion | flops 1179456 | bytes 787200 | tf_op jit(solution)/shard_map/reduce_sum | solution.py:16
  19.3 0.1 fusion.35
  19.5 1.6 %all-to-all-done = f32[8,2,768]{2,1,0:T(2,128)S(1)} async-done(((f32[8,2,768]{2,1,0:T(2,128)}), f32[8,2,768]{2,1,0:T(2,128)S(1)}, u32[]{:S(2)}, u32[]{:S(2)}) %all-to-all-start) | async-done | bytes 49184 | tf_op jit(solution)/shard_map/all_to_all | solution.py:92
  21.1 0.5 convolution_convert_fusion.1
  21.6 0.5 convolution_convert_fusion.2
  22.2 31.1 %all-gather = bf16[8,30,2048]{2,1,0:T(8,128)(2,1)S(1)} all-gather(bf16[1,30,2048]{2,1,0:T(8,128)(2,1)S(1)} %fusion.19), channel_id=1, replica_groups=mesh['sp'=4,'tp'=8] {'tp'}, dimensions={0}, use_global_device_ids=true | all-gather | bytes 1105920 | tf_op jit(solution)/shard_map/all_gather | solution.py:99
  53.3 0.3 reshape.365
  53.6 1.5 %convolution_convert_fusion = bf16[240,128]{1,0:T(8,128)(2,1)S(1)} fusion(bf16[240,2048]{1,0:T(8,128)(2,1)S(1)} %reshape.365, bf16[2048,128]{1,0:T(8,128)(2,1)} %param.17), kind=kOutput, calls=%fused_computation.13 | convolution fusion | flops 125859840 | bytes 1568768 | tf_op jit(solution)/shard_map/dot_general | solution.py:104
  55.1 1.4 %fusion.49 = f32[240,128]{1,0:T(8,128)S(1)} fusion(bf16[240,2048]{1,0:T(8,128)(2,1)S(1)} %reshape.365, bf16[2048,128]{1,0:T(8,128)(2,1)} %param.16), kind=kOutput, calls=%fused_computation.87 | convolution fusion | flops 125829120 | bytes 1630208 | tf_op jit(solution)/shard_map/dot_general | solution.py:103
  56.5 0.4 fusion.48
  57.6 6.3 %all_gather.10 = bf16[1728,128]{1,0:T(8,128)(2,1)S(1)} all-gather(bf16[432,128]{1,0:T(8,128)(2,1)S(1)} %pad_maximum_fusion), channel_id=1, replica_groups=mesh['sp'=4,'tp'=8] {'sp'}, dimensions={0}, use_global_device_ids=true | all-gather | bytes 552960 | tf_op jit(solution)/shard_map/all_gather | solution.py:127
  63.9 0.2 copy.28
  64.1 6.8 %all_gather.11 = bf16[1728,128]{1,0:T(8,128)(2,1)S(1)} all-gather(bf16[432,128]{1,0:T(8,128)(2,1)S(1)} %pad_maximum_fusion.1), channel_id=1, replica_groups=mesh['sp'=4,'tp'=8] {'sp'}, dimensions={0}, use_global_device_ids=true | all-gather | bytes 552960 | tf_op jit(solution)/shard_map/all_gather | solution.py:128
  71.0 0.7 fusion.47
  71.7 0.6 fusion.1
  72.3 0.7 fusion.10
  73.0 0.2 fusion.27
  73.2 0.1 copy-done.6
  73.4 0.5 fusion.28
  73.9 48.4 %fusion = f32[32,2048]{1,0:T(8,128)S(1)} fusion(f32[240,2048]{1,0:T(8,128)S(1)} %fusion.28), kind=kCustom, calls=%all-reduce-scatter | all-reduce-scatter fusion | flops 524289 | bytes 2228736
  122.3 1.9 %collective-permute-start = (f32[14,2048]{1,0:T(8,128)S(1)}, f32[14,2048]{1,0:T(8,128)S(1)}, u32[]{:S(2)}, u32[]{:S(2)}) collective-permute-start(f32[14,2048]{1,0:T(8,128)S(1)} %slice.97), channel_id=1, source_target_pairs={{0,1},{1,2},{2,3},{3,4},{4,5},{5,6},{6,7},{8,9},{9,10},{10,11},{11... | collective-permute-start | bytes 344072
  124.2 0.6 dynamic-slice.4
  125.4 4.6 %collective-permute-done = f32[14,2048]{1,0:T(8,128)S(1)} collective-permute-done((f32[14,2048]{1,0:T(8,128)S(1)}, f32[14,2048]{1,0:T(8,128)S(1)}, u32[]{:S(2)}, u32[]{:S(2)}) %collective-permute-start) | collective-permute-done | bytes 114720
  130.0 0.2 concatenate.28
  130.3 0.2 multiply_reduce_fusion
  130.4 0.8 fusion.18
  (38 shorter events, 1.0 us)
Async XLA Ops:
  0.0 1.1 copy-start
  0.0 21.1 %copy-start.2 = (bf16[192,2048]{1,0:T(8,128)(2,1)S(1)}, bf16[192,2048]{1,0:T(8,128)(2,1)}, u32[]{:S(2)}) copy-start(bf16[192,2048]{1,0:T(8,128)(2,1)} %param.11) | copy-start | bytes 2359300
  0.0 21.1 %copy-start.3 = (bf16[2048,128]{1,0:T(8,128)(2,1)S(1)}, bf16[2048,128]{1,0:T(8,128)(2,1)}, u32[]{:S(2)}) copy-start(bf16[2048,128]{1,0:T(8,128)(2,1)} %param.17) | copy-start | bytes 1572868
  9.7 11.3 %all-to-all-start = ((f32[8,2,768]{2,1,0:T(2,128)}), f32[8,2,768]{2,1,0:T(2,128)S(1)}, u32[]{:S(2)}, u32[]{:S(2)}) async-start(f32[8,2,768]{2,1,0:T(2,128)} %stack.11), calls=%async_computation | async-start | bytes 98304 | tf_op jit(solution)/shard_map/all_to_all | solution.py:92
  16.6 4.9 %copy-start.4 = (bf16[2048,128]{1,0:T(8,128)(2,1)S(1)}, bf16[2048,128]{1,0:T(8,128)(2,1)}, u32[]{:S(2)}) copy-start(bf16[2048,128]{1,0:T(8,128)(2,1)} %param.16) | copy-start | bytes 1572868
  21.1 1.0 copy-start.1
  53.5 3.0 %copy-start.5 = (bf16[2048,128]{1,0:T(8,128)(2,1)S(1)}, bf16[2048,128]{1,0:T(8,128)(2,1)}, u32[]{:S(2)}) copy-start(bf16[2048,128]{1,0:T(8,128)(2,1)} %param.15) | copy-start | bytes 1572868
  72.3 1.0 copy-start.6
  73.4 50.8 %copy-start.7 = (u32[32]{0:T(128)S(1)}, u32[32]{0:T(128)}, u32[]{:S(2)}) copy-start(u32[32]{0:T(128)} %constant.70) | copy-start | bytes 388
  122.3 7.8 %collective-permute-start = (f32[14,2048]{1,0:T(8,128)S(1)}, f32[14,2048]{1,0:T(8,128)S(1)}, u32[]{:S(2)}, u32[]{:S(2)}) collective-permute-start(f32[14,2048]{1,0:T(8,128)S(1)} %slice.97), channel_id=1, source_target_pairs={{0,1},{1,2},{2,3},{3,4},{4,5},{5,6},{6,7},{8,9},{9,10},{10,11},{11... | collective-permute-start | bytes 344072
